TPU v7x, 32 devices: a whole 2x2x4 slice. The times are simulated.
32 devices in a mesh: ep: 16 (over z, y, x), tp: 2 (over core).
Axes of the slice: x: 2, y: 2, z: 4, core: 2. Of those that a mesh axis runs over, the one named last changes fastest.
Arguments:
- tokens: bfloat16 [512, 2048], P('ep'), may hold values from -6 to 6
- lengths: int32 [512], P('ep'), may hold values from 128 to 1024
- key_cache: bfloat16 [512, 1024, 256], P('ep', None, 'tp'), may hold values from -1000 to 1000
- value_cache: bfloat16 [512, 1024, 256], P('ep', None, 'tp'), may hold values from -6 to 6
- gate_cache: float32 [512, 16, 1024], P('ep', 'tp'), may hold values from -130 to 0, as said below
- mix_gain: float32 [2048], replicated, may hold values from 0.1 to 1.9
- query_weight: bfloat16 [2048, 1024], P(None, 'tp'), may hold values from -0.125 to 0.125
- key_weight: bfloat16 [2048, 256], P(None, 'tp'), may hold values from -0.125 to 0.125
- value_weight: bfloat16 [2048, 256], P(None, 'tp'), may hold values from -0.125 to 0.125
- forget_weight: bfloat16 [2048, 16], P(None, 'tp'), may hold values from -0.125 to 0.125
- out_weight: bfloat16 [1024, 2048], P('tp'), may hold values from -0.1875 to 0.1875
- expert_gain: float32 [2048], replicated, may hold values from 0.1 to 1.9
- routes: int32 [512, 2], P('ep'), may hold values from 0 to 7, all different within a row; in each aligned block of 32 rows (0 to 31, 32 to 63, ...) at most 12 rows name the same one
- route_weights: float32 [512, 2], P('ep'), may hold values from 0.2 to 1
- expert_gate: bfloat16 [2048, 65536], P(None, ('ep', 'tp')), may hold values from -0.125 to 0.125
- expert_up: bfloat16 [2048, 65536], P(None, ('ep', 'tp')), may hold values from -0.125 to 0.125
- expert_down: bfloat16 [65536, 2048], P(('ep', 'tp')), may hold values from -0.0625 to 0.0625
Outputs:
- layer_out: bfloat16 [512, 2048], P('ep')
Inputs may be any that keep to these rules, and one draw needn't show every extreme that they name: `routes`: within the rows of one index of ep, no expert is named more than 12 times, and in every draw some expert is named exactly 12 times in some such rows; the 2 experts of a row differ. `gate_cache`: for each sequence and head the values never rise along the cache positions.
All inputs are finite; a program needn't handle non-finite values.
Results may differ from a plain program's by a relative error of at most 0.013.
Values may be sent and summed in bfloat16 or wider, within the bound.
A program may use at most 128 MiB of HBM per device.

v0:
```python
import jax
import jax.numpy as jnp
from jax import lax
from jax.sharding import PartitionSpec as P

HD = 64
EXPERTS = 8
CAP = 12


eps = 1e-06


def normed(values, gain):
    floats = values.astype(jnp.float32)
    return floats * lax.rsqrt(jnp.mean(floats * floats, axis=-1, keepdims=True) + eps) * gain


def attend(queries, key_new, value_new, log_gate, key_rows, value_rows, cumulative, length):
    seq_count, head_count, head_size = queries.shape
    kv_count = key_new.shape[1]
    group_size = head_count // kv_count
    cache_locations = key_rows.shape[1]
    factor = head_size ** (-0.5)
    grouped = queries.reshape(seq_count, kv_count, group_size, head_size)
    key_split = key_rows.reshape(seq_count, cache_locations, kv_count, head_size)
    value_split = value_rows.reshape(seq_count, cache_locations, kv_count, head_size)
    scores = (
        jnp.einsum(
            "skgd,spkd->skgp", grouped, key_split, preferred_element_type=jnp.float32
        ).reshape(seq_count, head_count, cache_locations)
        * factor
    )
    positions = jnp.arange(cache_locations, dtype=jnp.int32)
    latest = jnp.sum(
        jnp.where(positions[None, None, :] == (length - 1)[:, None, None], cumulative, 0.0), axis=-1
    )
    scores = scores + (latest + log_gate)[..., None] - cumulative
    valid = positions[None, None, :] < length[:, None, None]
    scores = jnp.where(valid, scores, -jnp.inf)
    own_score = (
        jnp.einsum("skgd,skd->skg", grouped, key_new, preferred_element_type=jnp.float32).reshape(
            seq_count, head_count
        )
        * factor
    )
    highest = jnp.maximum(jnp.max(scores, axis=-1), own_score)
    raised = jnp.exp(scores - highest[..., None])
    own_raised = jnp.exp(own_score - highest)
    denominator = jnp.sum(raised, axis=-1) + own_raised
    weights = (raised / denominator[..., None]).astype(jnp.bfloat16)
    own_weight = (own_raised / denominator).astype(jnp.bfloat16)
    mixed = jnp.einsum(
        "skgp,spkd->skgd",
        weights.reshape(seq_count, kv_count, group_size, cache_locations),
        value_split,
        preferred_element_type=jnp.float32,
    )
    mixed = (
        mixed
        + own_weight.reshape(seq_count, kv_count, group_size)[..., None].astype(jnp.float32)
        * value_new.astype(jnp.float32)[:, :, None, :]
    )
    return mixed.reshape(seq_count, head_count * head_size).astype(jnp.bfloat16)


def expert_work(rows_in, expert_gate, expert_up, expert_down):
    leading = rows_in.shape[:-1]
    flat_rows = rows_in.reshape(-1, rows_in.shape[-1])
    gate_out = jnp.dot(flat_rows, expert_gate, preferred_element_type=jnp.float32)
    up_out = jnp.dot(flat_rows, expert_up, preferred_element_type=jnp.float32)
    hidden = (jax.nn.silu(gate_out) * up_out).astype(jnp.bfloat16)
    return jnp.dot(hidden, expert_down, preferred_element_type=jnp.float32).reshape(
        leading + (expert_down.shape[1],)
    )


def combine(returned, target, route_weights):
    capacity = returned.shape[1]
    columns = returned.shape[2]
    blocks = jnp.sum(
        returned.reshape(EXPERTS, -1, capacity, columns).astype(jnp.float32), axis=1
    ).reshape(EXPERTS * capacity, columns)
    picked = jnp.take(blocks, target, axis=0).reshape(route_weights.shape + (columns,))
    return jnp.sum(picked * route_weights[..., None], axis=1)


def on_device(
    tokens,
    lengths,
    key_cache,
    value_cache,
    gate_cache,
    mix_gain,
    query_weight,
    key_weight,
    value_weight,
    forget_weight,
    out_weight,
    expert_gain,
    routes,
    route_weights,
    expert_gate,
    expert_up,
    expert_down,
):
    seq_count = tokens.shape[0]
    width = tokens.shape[1]
    normal_in = normed(tokens, mix_gain).astype(jnp.bfloat16)
    queries = (
        jnp.dot(normal_in, query_weight, preferred_element_type=jnp.float32)
        .astype(jnp.bfloat16)
        .reshape(seq_count, -1, HD)
    )
    key_new = (
        jnp.dot(normal_in, key_weight, preferred_element_type=jnp.float32)
        .astype(jnp.bfloat16)
        .reshape(seq_count, -1, HD)
    )
    value_new = (
        jnp.dot(normal_in, value_weight, preferred_element_type=jnp.float32)
        .astype(jnp.bfloat16)
        .reshape(seq_count, -1, HD)
    )
    log_gate = jax.nn.log_sigmoid(
        jnp.dot(normal_in, forget_weight, preferred_element_type=jnp.float32)
    )
    mixed = attend(
        queries, key_new, value_new, log_gate, key_cache, value_cache, gate_cache, lengths
    )
    partial_out = jnp.dot(mixed, out_weight, preferred_element_type=jnp.float32).astype(
        jnp.bfloat16
    )
    residual = (
        tokens.astype(jnp.float32) + lax.psum(partial_out, "tp").astype(jnp.float32)
    ).astype(jnp.bfloat16)
    expert_in = normed(residual, expert_gain).astype(jnp.bfloat16)
    top_count = routes.shape[1]
    flat_routes = routes.reshape(-1)
    one_hot = (flat_routes[:, None] == jnp.arange(EXPERTS, dtype=jnp.int32)[None, :]).astype(
        jnp.int32
    )
    slot_index = jnp.sum((jnp.cumsum(one_hot, axis=0) - 1) * one_hot, axis=1)
    target = flat_routes * CAP + slot_index
    dispatch = (jnp.arange(EXPERTS * CAP, dtype=jnp.int32)[:, None] == target[None, :]).astype(
        jnp.bfloat16
    )
    repeated = jnp.repeat(expert_in, top_count, axis=0)
    outgoing = jnp.dot(dispatch, repeated, preferred_element_type=jnp.float32).astype(jnp.bfloat16)
    pieces = lax.axis_size("ep") // EXPERTS
    outgoing = jnp.broadcast_to(
        outgoing.reshape(EXPERTS, 1, CAP, width), (EXPERTS, pieces, CAP, width)
    ).reshape(EXPERTS * pieces, CAP, width)
    half_width = width // lax.axis_size("tp")
    start = lax.axis_index("tp") * half_width
    outgoing_half = lax.dynamic_slice_in_dim(outgoing, start, half_width, 2)
    full_rows = lax.all_gather(
        lax.all_to_all(outgoing_half, "ep", split_axis=0, concat_axis=0, tiled=True),
        "tp",
        axis=2,
        tiled=True,
    )
    partial_rows = expert_work(full_rows, expert_gate, expert_up, expert_down).astype(jnp.bfloat16)
    share = (
        lax.psum_scatter(partial_rows, "tp", scatter_dimension=2, tiled=True)
        .astype(jnp.float32)
        .astype(jnp.bfloat16)
    )
    returned = lax.all_to_all(share, "ep", split_axis=0, concat_axis=0, tiled=True)
    mixture = combine(returned, target, route_weights)
    own_half = lax.dynamic_slice_in_dim(residual, start, half_width, 1).astype(jnp.float32)
    return lax.all_gather((own_half + mixture).astype(jnp.bfloat16), "tp", axis=1, tiled=True)


def solution(mesh):
    return jax.shard_map(
        on_device,
        mesh=mesh,
        in_specs=(
            P("ep", None),
            P("ep"),
            P("ep", None, "tp"),
            P("ep", None, "tp"),
            P("ep", "tp", None),
            P(),
            P(None, "tp"),
            P(None, "tp"),
            P(None, "tp"),
            P(None, "tp"),
            P("tp", None),
            P(),
            P("ep", None),
            P("ep", None),
            P(None, ("ep", "tp")),
            P(None, ("ep", "tp")),
            P(("ep", "tp"), None),
        ),
        out_specs=P("ep", None),
        check_vma=False,
    )
```

profile of v0, /device:TPU:0, one launch (start us, length us, event | category | flops | bytes accessed | tf_op | source)
XLA Modules:
  0.0 167.7 jit_solution(255999665573253015)
XLA Ops:
  9.1 2.2 %convolution_convert_fusion.3 = bf16[32,512]{1,0:T(8,128)(2,1)S(1)} fusion(bf16[2048,512]{1,0:T(8,128)(2,1)} %param.23, bf16[32,2048]{1,0:T(8,128)(2,1)} %param.17, f32[2048]{0:T(1024)} %param.22, f32[32]{0:T(128)S(1)} %add_rsqrt_fusion.1), kind=kOutput, calls=%fused_computation.9 | convolution fusion | flops 67387392 | bytes 2269312 | tf_op jit(solution)/shard_map/dot_general | solution.py:111
  11.5 11.9 %copy.45 = bf16[32,1024,128]{1,2,0:T(8,128)(2,1)} copy(bf16[32,1024,128]{2,1,0:T(8,128)(2,1)} %param.19) | data formatting | bytes 16777216 | tf_op args[2]
  23.4 4.6 %convolution_multiply_fusion.1 = f32[32,2,4,1024]{3,2,1,0:T(4,128)S(1)} fusion(bf16[32,2,4,64]{3,2,1,0:T(4,128)(2,1)S(1)} %reshape_reshape.3, bf16[32,1024,2,64]{1,3,2,0:T(8,128)(2,1)} %bitcast.37), kind=kOutput, calls=%fused_computation.6 | convolution fusion | flops 33816576 | bytes 9469952 | tf_op jit(solution)/shard_map/skgd,spkd->skgp/dot_general | solution.py:29
  28.0 1.4 mul.132
  29.5 1.5 select_reduce_fusion
  31.3 1.9 %fusion.25 = (f32[32,8]{1,0:T(8,128)S(1)}, f32[32,8,1024]{2,1,0:T(8,128)S(1)}) fusion(f32[32,8,1024]{2,1,0:T(8,128)} %param.21, f32[32,8,1024]{2,1,0:T(8,128)} %mul.132, f32[32,8]{1,0:T(8,128)S(1)} %copy.47, pred[32,1024]{1,0:T(8,128)(4,1)S(1)} %iota_compare_fusion.1), kind=kLoop, calls=%fused_computation.64 | loop fusion | flops 1048320 | bytes 3180544 | tf_op jit(solution)/shard_map/reduce_max | solution.py:47
  33.3 1.3 convolution_convert_fusion.5
  35.5 1.1 divide_convert_fusion
  36.6 1.2 reshape.188
  38.0 1.3 fusion.2
  39.4 11.9 %copy.52 = bf16[32,1024,128]{1,2,0:T(8,128)(2,1)} copy(bf16[32,1024,128]{2,1,0:T(8,128)(2,1)} %param.20) | data formatting | bytes 16777216 | tf_op args[3]
  51.3 5.7 %fusion.1 = bf16[32,2,4,64]{3,2,1,0:T(4,128)(2,1)S(1)} fusion(bf16[32,2,4,1024]{3,2,1,0:T(4,128)(2,1)S(1)} %reshape.188, bf16[32,1024,2,64]{1,3,2,0:T(8,128)(2,1)} %bitcast.38, f32[32,2,64]{2,1,0:T(2,128)S(1)} %reshape.195, f32[32,2,4]{2,1,0:T(2,128)S(1)} %copy.55), kind=kOutput, calls=%fused_computation.8 | convolution fusion | flops 33603584 | bytes 8963072 | tf_op jit(solution)/shard_map/skgp,spkd->skgd/dot_general | solution.py:53
  57.1 1.1 convolution_convert_fusion.2
  58.9 20.2 %all-reduce.2.cloned.1.call-done = bf16[32,2048]{1,0:T(8,128)(2,1)} async-done(((bf16[32,2048]{1,0:T(8,128)(2,1)}), bf16[32,2048]{1,0:T(8,128)(2,1)}) %all-reduce.2.cloned.1.call-update) | async-done | bytes 131088 | tf_op jit(solution)/shard_map/psum | solution.py:135
  81.6 22.1 %all_to_all.10 = bf16[16,12,1024]{2,1,0:T(8,128)(2,1)S(1)} all-to-all(bf16[16,12,1024]{2,1,0:T(8,128)(2,1)S(1)} %constant_dynamic-slice_fusion), channel_id=1, replica_groups=mesh['ep'=16,'tp'=2] {'ep'}, dimensions={0} | all-to-all | bytes 786432 | tf_op jit(solution)/shard_map/all_to_all | solution.py:158
  103.7 2.7 %all_gather.6 = bf16[16,12,2048]{2,1,0:T(8,128)(2,1)S(1)} all-gather(bf16[16,12,1024]{2,1,0:T(8,128)(2,1)S(1)} %all_to_all.10), channel_id=1, replica_groups=mesh['ep'=16,'tp'=2] {'tp'}, dimensions={2}, use_global_device_ids=true | all-gather | bytes 1179648 | tf_op jit(solution)/shard_map/all_gather | solution.py:157
  106.6 6.3 %fusion.27 = f32[192,2048]{1,0:T(8,128)} fusion(bf16[192,2048]{1,0:T(8,128)(2,1)S(1)} %reshape.193, bf16[2048,2048]{1,0:T(8,128)(2,1)} %param.31), kind=kOutput, calls=%fused_computation.66 | convolution fusion | flops 1610612736 | bytes 10747904 | tf_op jit(solution)/shard_map/dot_general | solution.py:70
  113.0 10.9 %convolution_convert_fusion = bf16[192,2048]{1,0:T(8,128)(2,1)} fusion(bf16[2048,2048]{1,0:T(8,128)(2,1)} %param.33, bf16[192,2048]{1,0:T(8,128)(2,1)S(1)} %reshape.193, bf16[2048,2048]{1,0:T(8,128)(2,1)} %param.32, f32[192,2048]{1,0:T(8,128)} %fusion.27), kind=kOutput, calls=%fused_computation.2 | convolution fusion | flops 3223977984 | bytes 19922944 | tf_op jit(solution)/shard_map/dot_general | solution.py:73
  123.8 2.1 %convert_element_type.110 = bf16[16,12,2048]{2,1,0:T(8,128)(2,1)} reshape(bf16[192,2048]{1,0:T(8,128)(2,1)} %convolution_convert_fusion) | data formatting | bytes 1572864 | tf_op jit(solution)/shard_map/convert_element_type | solution.py:163
  126.1 6.8 %reduce-scatter.2.cloned.1.call-done = bf16[16,12,1024]{2,1,0:T(8,128)(2,1)} async-done(((bf16[16,12,2048]{2,1,0:T(8,128)(2,1)}), bf16[16,12,1024]{2,1,0:T(8,128)(2,1)}) %reduce-scatter.2.cloned.1.call-update) | async-done | bytes 393232 | tf_op jit(solution)/shard_map/reduce_scatter | solution.py:165
  132.9 6.8 %all-to-all-start.1 = ((bf16[16,12,1024]{2,1,0:T(8,128)(2,1)}), bf16[16,12,1024]{2,1,0:T(8,128)(2,1)S(1)}, u32[]{:S(2)}, u32[]{:S(2)}) async-start(bf16[16,12,1024]{2,1,0:T(8,128)(2,1)} %reduce-scatter.2.cloned.1.call-done), calls=%async_computation.2 | async-start | bytes 1048576 | tf_op jit(solution)/shard_map/all_to_all | solution.py:169
  141.3 13.8 %all-to-all-done.1 = bf16[16,12,1024]{2,1,0:T(8,128)(2,1)S(1)} async-done(((bf16[16,12,1024]{2,1,0:T(8,128)(2,1)}), bf16[16,12,1024]{2,1,0:T(8,128)(2,1)S(1)}, u32[]{:S(2)}, u32[]{:S(2)}) %all-to-all-start.1) | async-done | bytes 393248 | tf_op jit(solution)/shard_map/all_to_all | solution.py:169
  156.3 1.2 multiply_reduce_fusion
  158.3 1.9 %all_gather.7 = bf16[32,2048]{1,0:T(8,128)(2,1)S(1)} all-gather(bf16[32,1024]{1,0:T(8,128)(2,1)S(1)} %add_convert_fusion), channel_id=1, replica_groups=mesh['ep'=16,'tp'=2] {'tp'}, dimensions={1}, use_global_device_ids=true | all-gather | bytes 196608 | tf_op jit(solution)/shard_map/all_gather | solution.py:172
  (78 shorter events, 12.2 us)
Async XLA Ops:
  6.5 50.6 %copy-start = (bf16[512,2048]{1,0:T(8,128)(2,1)S(1)}, bf16[512,2048]{1,0:T(8,128)(2,1)}, u32[]{:S(2)}) copy-start(bf16[512,2048]{1,0:T(8,128)(2,1)} %param.27) | copy-start | bytes 6291460
  6.5 72.6 %all-reduce.2.cloned.1.call-start = ((), (), s32[]{:S(2)}) async-start(), calls=%async_computation.3 | async-start | bytes 262144 | tf_op jit(solution)/shard_map/psum | solution.py:135
  23.4 7.6 %copy-start.2 = (bf16[32,2048]{1,0:T(8,128)(2,1)S(1)}, bf16[32,2048]{1,0:T(8,128)(2,1)}, u32[]{:S(2)}) copy-start(bf16[32,2048]{1,0:T(8,128)(2,1)} %param.17) | copy-start | bytes 393220
  23.4 7.6 %copy-start.4 = (f32[2048]{0:T(1024)S(1)}, f32[2048]{0:T(1024)}, u32[]{:S(2)}) copy-start(f32[2048]{0:T(1024)} %param.22) | copy-start | bytes 24580
  23.4 7.6 %copy-start.8 = (bf16[2048,8]{0,1:T(8,128)(2,1)S(1)}, bf16[2048,8]{0,1:T(8,128)(2,1)}, u32[]{:S(2)}) copy-start(bf16[2048,8]{0,1:T(8,128)(2,1)} %param.26) | copy-start | bytes 98308
  51.3 7.0 %copy-start.5 = (s32[32,2]{0,1:T(2,128)S(1)}, s32[32,2]{0,1:T(2,128)}, u32[]{:S(2)}) copy-start(s32[32,2]{0,1:T(2,128)} %param.29) | copy-start | bytes 772
  51.3 28.9 %copy-start.6 = (f32[2048]{0:T(1024)S(1)}, f32[2048]{0:T(1024)}, u32[]{:S(2)}) copy-start(f32[2048]{0:T(1024)} %param.28) | copy-start | bytes 24580
  58.3 74.6 %reduce-scatter.2.cloned.1.call-start = ((), (), s32[]{:S(2)}) async-start(), calls=%async_computation.4 | async-start | bytes 1572864 | tf_op jit(solution)/shard_map/reduce_scatter | solution.py:165
  80.2 0.7 copy-start.3
  113.0 27.7 %copy-start.7 = (f32[32,2]{0,1:T(2,128)S(1)}, f32[32,2]{0,1:T(2,128)}, u32[]{:S(2)}) copy-start(f32[32,2]{0,1:T(2,128)} %param.30) | copy-start | bytes 772
  113.0 47.9 %copy-start.1 = (bf16[512,2048]{1,0:T(8,128)(2,1)S(1)}, bf16[512,2048]{1,0:T(8,128)(2,1)}, u32[]{:S(2)}) copy-start(bf16[512,2048]{1,0:T(8,128)(2,1)} %param.27) | copy-start | bytes 6291460
  132.9 22.3 %all-to-all-start.1 = ((bf16[16,12,1024]{2,1,0:T(8,128)(2,1)}), bf16[16,12,1024]{2,1,0:T(8,128)(2,1)S(1)}, u32[]{:S(2)}, u32[]{:S(2)}) async-start(bf16[16,12,1024]{2,1,0:T(8,128)(2,1)} %reduce-scatter.2.cloned.1.call-done), calls=%async_computation.2 | async-start | bytes 1048576 | tf_op jit(solution)/shard_map/all_to_all | solution.py:169
Sparse Core Ops, SparseCore 0:
  58.4 20.6 all-reduce.1
  126.1 6.7 reduce-scatter.1
where the time goes:
time: 169 us; the launch traced here: 168 us
  waiting for transfers between devices  40.8 us (24%)
  matrix products  34.1 us (20%)
  local copies, waits for them, and re-layouts  33.9 us (20%)
  blocking collectives  26.7 us (16%)
  between operations  13.7 us (8%)
  other arithmetic  11.7 us (7%)
  starting transfers between devices  6.82 us (4%)
    unnamed x23, local copies, waits for them, and re-layouts  25.3 us
    all_to_all x1, blocking collectives, on_device(): lax.all_to_all(outgoing_half, 'ep', split_axis=0, concat_axis=0, tiled=True)  22.1 us
    psum x1, waiting for transfers between devices, on_device(): lax.psum(partial_out, 'tp').astype(jnp.float32)  20.2 us
    all_to_all x1, waiting for transfers between devices, on_device(): lax.all_to_all(share, 'ep', split_axis=0, concat_axis=0, tiled=True)  13.8 us
    dot_general x1, matrix products, expert_work(): jnp.dot(hidden, expert_down, preferred_element_type=jnp.float32)  10.9 us
    all_to_all x1, starting transfers between devices, on_device(): lax.all_to_all(share, 'ep', split_axis=0, concat_axis=0, tiled=True)  6.78 us
    reduce_scatter x1, waiting for transfers between devices, on_device(): lax.psum_scatter(partial_rows, 'tp', scatter_dimension=2, tiled=True)  6.77 us
    dot_general x1, matrix products, expert_work(): jnp.dot(flat_rows, expert_gate, preferred_element_type=jnp.float32)  6.34 us
  transfers between devices with their start and end apart: 3, of which 3 were waited for; matrix products, arithmetic and copies ran while one was open for 1% of the time, Pallas kernels for 0%

commit v1 on v0

v1 whole, which is shorter than its diff:
```python
import functools

import jax
import jax.numpy as jnp
from jax import lax
from jax.experimental import pallas as pl
from jax.experimental.pallas import tpu as pltpu
from jax.sharding import PartitionSpec as P

HD = 64
EXPERTS = 8
CAP = 12
QUARTERS = 4
GROUP = 4
STEP_SEQS = 4
MESH = pl.DeviceIdType.MESH
F32 = jnp.float32
BF16 = jnp.bfloat16

eps = 1e-06


def normed(values, gain):
    floats = values.astype(F32)
    return floats * lax.rsqrt(jnp.mean(floats * floats, axis=-1, keepdims=True) + eps) * gain


def attention_kernel(
    len_ref, tok_ref, gain_ref, wq_ref, wk_ref, wv_ref, wf_ref, wo_ref, k_ref, v_ref, g_ref,
    out_ref, q_sc, lg_sc, kn_sc, vn_sc, mix_sc,
):
    step = pl.program_id(0)
    seqs = tok_ref.shape[0]
    heads = g_ref.shape[1]
    lanes = k_ref.shape[2]
    positions = k_ref.shape[1]
    group = heads // (lanes // HD)
    per_slice = lanes // HD
    lane = lax.broadcasted_iota(jnp.int32, (seqs, lanes), 1)

    @pl.when(step == 0)
    def _():
        x = normed(tok_ref[...], gain_ref[...]).astype(BF16)
        q = jnp.dot(x, wq_ref[...], preferred_element_type=F32).astype(BF16).astype(F32)
        kn_sc[...] = jnp.dot(x, wk_ref[...], preferred_element_type=F32).astype(BF16).astype(F32)
        vn_sc[...] = jnp.dot(x, wv_ref[...], preferred_element_type=F32).astype(BF16).astype(F32)
        gates = jnp.dot(x, wf_ref[...], preferred_element_type=F32)
        gates = jnp.minimum(gates, 0.0) - jnp.log1p(jnp.exp(-jnp.abs(gates)))
        for h in range(heads):
            base = (h // per_slice) * lanes
            part = q[:, base:base + lanes]
            at, want = h % per_slice, h // group
            if at != want:
                part = pltpu.roll(part, (want - at) * HD % lanes, 1)
            part = jnp.where(lane // HD == want, part, 0.0)
            q_sc[:, h, :] = part
            lg_sc[:, h, :] = jnp.broadcast_to(gates[:, h:h + 1], (seqs, lanes))

    pos = lax.broadcasted_iota(jnp.int32, (heads, positions), 1)
    factor = HD ** (-0.5)
    for j in range(k_ref.shape[0]):
        s = step * k_ref.shape[0] + j
        length = len_ref[s]
        q = q_sc[s]
        g = g_ref[j]
        scores = lax.dot_general(
            q.astype(BF16), k_ref[j], (((1,), (1,)), ((), ())), preferred_element_type=F32
        ) * factor
        latest = jnp.sum(jnp.where(pos == length - 1, g, 0.0), axis=-1, keepdims=True)
        scores = scores + (latest + lg_sc[s][:, 0:1]) - g
        scores = jnp.where(pos < length, scores, -jnp.inf)
        own = jnp.sum(q * kn_sc[pl.ds(s, 1), :], axis=-1, keepdims=True) * factor
        top = jnp.maximum(jnp.max(scores, axis=-1, keepdims=True), own)
        raised = jnp.exp(scores - top)
        own_raised = jnp.exp(own - top)
        inverse = 1.0 / (jnp.sum(raised, axis=-1, keepdims=True) + own_raised)
        weights = (raised * inverse).astype(BF16)
        own_weight = (own_raised * inverse).astype(BF16).astype(F32)
        mix_sc[s] = (
            jnp.dot(weights, v_ref[j], preferred_element_type=F32)
            + own_weight * vn_sc[pl.ds(s, 1), :]
        )

    @pl.when(step == pl.num_programs(0) - 1)
    def _():
        pieces = []
        for base in range(0, heads, per_slice):
            joined = None
            for h in range(base, base + per_slice):
                part = mix_sc[:, h, :]
                at, want = h // group, h % per_slice
                if at != want:
                    part = pltpu.roll(part, (want - at) * HD % lanes, 1)
                joined = part if joined is None else jnp.where(lane // HD == want, part, joined)
            pieces.append(joined.astype(BF16))
        mixed = jnp.concatenate(pieces, axis=1)
        out_ref[...] = jnp.dot(mixed, wo_ref[...], preferred_element_type=F32).astype(BF16)


def attention(tokens, lengths, key_cache, value_cache, gate_cache, mix_gain, wq, wk, wv, wf, wo):
    seqs, width = tokens.shape
    _, positions, lanes = key_cache.shape
    heads = gate_cache.shape[1]
    whole = lambda a: pl.BlockSpec(a.shape, lambda i: (0,) * a.ndim)
    gain = mix_gain.reshape(1, width)
    return pl.pallas_call(
        attention_kernel,
        grid=(seqs // STEP_SEQS,),
        out_shape=jax.ShapeDtypeStruct((seqs, width), BF16),
        in_specs=[pl.BlockSpec(memory_space=pltpu.SMEM)]
        + [whole(a) for a in (tokens, gain, wq, wk, wv, wf, wo)]
        + [
            pl.BlockSpec((STEP_SEQS, positions, lanes), lambda i: (i, 0, 0)),
            pl.BlockSpec((STEP_SEQS, positions, lanes), lambda i: (i, 0, 0)),
            pl.BlockSpec((STEP_SEQS, heads, positions), lambda i: (i, 0, 0)),
        ],
        out_specs=pl.BlockSpec((seqs, width), lambda i: (0, 0)),
        scratch_shapes=[
            pltpu.VMEM((seqs, heads, lanes), F32),
            pltpu.VMEM((seqs, heads, lanes), F32),
            pltpu.VMEM((seqs, lanes), F32),
            pltpu.VMEM((seqs, lanes), F32),
            pltpu.VMEM((seqs, heads, lanes), F32),
        ],
        compiler_params=pltpu.CompilerParams(
            dimension_semantics=("arbitrary",), vmem_limit_bytes=48 * 1024 * 1024
        ),
        name="attention",
    )(lengths, tokens, gain, wq, wk, wv, wf, wo, key_cache, value_cache, gate_cache)


def moe_kernel(
    n_ep, part_ref, tok_ref, gain_ref, routes_ref, rw_ref, wg_hbm, wu_hbm, wd_hbm, out_ref,
    wg, wu, wd, peer_part, residual, normal, outgoing, rows, x_sc, h_sc, stage, s_other, s_own,
    t_in, blocks, u_in, finals, returned,
    w_sem, part_sem, col_send, fan_send, mate_send, row_recv, t_send, t_recv, u_send, u_recv,
    ret_send, ret_recv, out_sem,
):
    me = lax.axis_index("ep")
    t = lax.axis_index("tp")
    pieces = n_ep // EXPERTS
    e, p = me // pieces, lax.rem(me, pieces)
    mate = (me, 1 - t)
    order = (4, 3, 5, 2, 6, 1, 7)
    seqs, width = tok_ref.shape
    half = width // 2
    quarter = half // QUARTERS
    ff = wg_hbm.shape[1]

    def column(k):
        return lax.rem(e + k, EXPERTS)

    def peer(i):
        return lax.rem(p + i, pieces)

    weight_copies = [
        pltpu.make_async_copy(src, dst, w_sem.at[i])
        for i, (src, dst) in enumerate(((wg_hbm, wg), (wu_hbm, wu), (wd_hbm, wd)))
    ]
    for copy in weight_copies:
        copy.start()

    barrier = pltpu.get_barrier_semaphore()
    pl.semaphore_signal(barrier, inc=1, device_id=mate, device_id_type=MESH)
    for i in range(1, pieces):
        pl.semaphore_signal(barrier, inc=1, device_id=(e * pieces + peer(i), t), device_id_type=MESH)
    for k in range(1, EXPERTS):
        pl.semaphore_signal(barrier, inc=1, device_id=(column(k) * pieces + p, t), device_id_type=MESH)
    pl.semaphore_wait(barrier, 1 + (pieces - 1) + (EXPERTS - 1))

    def send(src, dst, send_sem, recv_sem, device):
        copy = pltpu.make_async_remote_copy(
            src_ref=src, dst_ref=dst, send_sem=send_sem, recv_sem=recv_sem,
            device_id=device, device_id_type=MESH,
        )
        copy.start()
        return copy

    def arrived(dst, send_sem, recv_sem):
        pltpu.make_async_remote_copy(
            src_ref=dst, dst_ref=dst, send_sem=send_sem, recv_sem=recv_sem,
            device_id=mate, device_id_type=MESH,
        ).wait_recv()

    sent = [send(part_ref, peer_part, part_sem.at[0], part_sem.at[1], mate)]

    block = QUARTERS * CAP
    columns = EXPERTS * block
    col = lax.broadcasted_iota(jnp.int32, (seqs, columns), 1)
    col_expert = col // block
    col_slot = lax.rem(col, CAP)
    r0, r1 = routes_ref[:, 0:1], routes_ref[:, 1:2]
    first, second = r0 == col_expert, r1 == col_expert
    named = jnp.where(first | second, 1.0, 0.0)
    before = jnp.where(
        lax.broadcasted_iota(jnp.int32, (seqs, seqs), 1)
        < lax.broadcasted_iota(jnp.int32, (seqs, seqs), 0), 1.0, 0.0,
    )
    slot = jnp.dot(before.astype(BF16), named.astype(BF16), preferred_element_type=F32)
    chosen = jnp.where(slot == col_slot.astype(F32), named, 0.0)
    weight = jnp.where(first, rw_ref[:, 0:1], jnp.where(second, rw_ref[:, 1:2], 0.0)) * chosen
    col_quarter = lax.rem(col, block) // CAP
    spread = lambda a: jnp.concatenate(
        [jnp.where(col_quarter == q, a, 0.0) for q in range(QUARTERS)], axis=0
    )
    dispatch = spread(chosen).astype(BF16)
    weight = spread(weight)
    weight_high = weight.astype(BF16)
    weight_low = (weight - weight_high.astype(F32)).astype(BF16)

    size = GROUP * block
    out_row = lax.broadcasted_iota(jnp.int32, (size, size), 0)
    in_row = lax.broadcasted_iota(jnp.int32, (size, size), 1)

    def unpacked(r):
        q = r // (GROUP * CAP)
        i = lax.rem(r, GROUP * CAP) // CAP
        return i * block + q * CAP + lax.rem(r, CAP)

    unpack = jnp.where(in_row == unpacked(out_row), 1.0, 0.0).astype(BF16)
    pack = jnp.where(out_row == unpacked(in_row), 1.0, 0.0).astype(BF16)

    arrived(peer_part, part_sem.at[0], part_sem.at[1])
    total = tok_ref[...].astype(F32) + (part_ref[...].astype(F32) + peer_part[...].astype(F32))
    rounded = total.astype(BF16)
    residual[...] = rounded
    normal[...] = normed(rounded, gain_ref[...]).astype(BF16)

    start = pl.multiple_of(t * half, half)
    mine = normal[:, pl.ds(start, half)]
    stacked = jnp.concatenate(
        [mine[:, q * quarter:(q + 1) * quarter] for q in range(QUARTERS)], axis=0
    )
    outgoing[...] = lax.dot_general(
        dispatch, stacked, (((0,), (0,)), ((), ())), preferred_element_type=F32
    ).astype(BF16).reshape(EXPERTS, block, quarter)

    own_row = p * EXPERTS + e
    for n, k in enumerate(order):
        a = column(k)
        sent.append(send(outgoing.at[a], rows.at[own_row, t], col_send.at[n],
                         row_recv.at[own_row, t], (a * pieces + p, t)))
    fans = 0
    mates = 0

    def fan(src, r):
        nonlocal fans
        for i in range(1, pieces):
            sent.append(send(src, rows.at[r, t], fan_send.at[fans], row_recv.at[r, t],
                             (e * pieces + peer(i), t)))
            fans += 1

    def to_mate(src, r):
        nonlocal mates
        sent.append(send(src, rows.at[r, t], mate_send.at[mates], row_recv.at[r, t], mate))
        mates += 1

    fan(outgoing.at[e], own_row)
    to_mate(outgoing.at[e], own_row)
    rows[own_row, t] = outgoing[e]
    inbound = [lax.rem(e + EXPERTS - k, EXPERTS) for k in order]
    for n, a in enumerate(inbound):
        r = p * EXPERTS + a
        arrived(rows.at[r, t], col_send.at[0], row_recv.at[r, t])
        fan(rows.at[r, t], r)
        to_mate(rows.at[r, t], r)
    for a in [e] + inbound:
        for i in range(1, pieces):
            r = peer(i) * EXPERTS + a
            arrived(rows.at[r, t], col_send.at[0], row_recv.at[r, t])
            to_mate(rows.at[r, t], r)
    for i in range(pieces):
        for a in [e] + inbound:
            r = peer(i) * EXPERTS + a
            arrived(rows.at[r, 1 - t], col_send.at[0], row_recv.at[r, 1 - t])

    groups = n_ep // GROUP
    group_rows = GROUP * CAP
    for g in range(groups):
        for h in range(2):
            packed = rows[g * GROUP:(g + 1) * GROUP, h].reshape(size, quarter)
            moved = jnp.dot(unpack, packed, preferred_element_type=F32).astype(BF16)
            for q in range(QUARTERS):
                x_sc[g * group_rows:(g + 1) * group_rows,
                     h * half + q * quarter:h * half + (q + 1) * quarter] = (
                    moved[q * group_rows:(q + 1) * group_rows])

    weight_copies[0].wait()
    weight_copies[1].wait()
    chunk = 256

    @pl.loop(0, ff // chunk)
    def _(c):
        at = pl.ds(pl.multiple_of(c * chunk, chunk), chunk)
        x = x_sc[...]
        gate = jnp.dot(x, wg[:, at], preferred_element_type=F32)
        up = jnp.dot(x, wu[:, at], preferred_element_type=F32)
        h_sc[:, at] = (gate * (1.0 / (1.0 + jnp.exp(-gate))) * up).astype(BF16)

    weight_copies[2].wait()

    def down(h, into):
        for q in range(QUARTERS):
            at = pl.ds(pl.multiple_of(h * half + q * quarter, quarter), quarter)
            y = jnp.dot(h_sc[...], wd[:, at], preferred_element_type=F32).astype(BF16)
            for g in range(groups):
                stage[g, q * group_rows:(q + 1) * group_rows] = (
                    y[g * group_rows:(g + 1) * group_rows])
        for g in range(groups):
            into[g * GROUP:(g + 1) * GROUP] = jnp.dot(
                pack, stage[g], preferred_element_type=F32
            ).astype(BF16).reshape(GROUP, block, quarter)

    down(1 - t, s_other)
    turns = list(range(1, pieces)) + [0]
    for i in turns:
        at = pl.ds(peer(i) * EXPERTS, EXPERTS)
        sent.append(send(s_other.at[at], t_in.at[at], t_send.at[i], t_recv.at[i], mate))
    down(t, s_own)
    backward = [column(k) for k in order] + [e]
    for i in turns:
        at = pl.ds(peer(i) * EXPERTS, EXPERTS)
        arrived(t_in.at[at], t_send.at[0], t_recv.at[i])
        for n, a in enumerate(backward):
            r = peer(i) * EXPERTS + a
            blocks[r] = (s_own[r].astype(F32) + t_in[r].astype(F32)).astype(BF16)
            if i > 0:
                sent.append(send(blocks.at[r], u_in.at[i - 1, a], u_send.at[i - 1, n],
                                 u_recv.at[i - 1, a], (e * pieces + peer(i), t)))
    for n, a in enumerate(backward):
        summed = blocks[p * EXPERTS + a].astype(F32)
        for i in range(1, pieces):
            arrived(u_in.at[i - 1, a], u_send.at[0, 0], u_recv.at[i - 1, a])
            summed = summed + u_in[i - 1, a].astype(F32)
        finals[a] = summed.astype(BF16)
        if n < len(order):
            sent.append(send(finals.at[a], returned.at[e], ret_send.at[n], ret_recv.at[e],
                             (a * pieces + p, t)))
    returned[e] = finals[e]
    for a in inbound:
        arrived(returned.at[a], ret_send.at[0], ret_recv.at[a])
    back = returned[...].reshape(columns, quarter)
    mixture = (
        jnp.dot(weight_high, back, preferred_element_type=F32)
        + jnp.dot(weight_low, back, preferred_element_type=F32)
    )
    for q in range(QUARTERS):
        at = pl.ds(pl.multiple_of(start + q * quarter, quarter), quarter)
        out_ref[:, at] = (
            residual[:, at].astype(F32) + mixture[q * seqs:(q + 1) * seqs]
        ).astype(BF16)
    here = pl.ds(start, half)
    there = pl.ds(pl.multiple_of((1 - t) * half, half), half)
    sent.append(send(out_ref.at[:, here], out_ref.at[:, here], out_sem.at[0], out_sem.at[1], mate))
    arrived(out_ref.at[:, there], out_sem.at[0], out_sem.at[1])
    for copy in sent:
        copy.wait_send()


def moe(n_ep, partial, tokens, expert_gain, routes, route_weights, gate, up, down):
    seqs, width = tokens.shape
    pieces = n_ep // EXPERTS
    half = width // 2
    quarter = half // QUARTERS
    block = QUARTERS * CAP
    ff = gate.shape[1]
    count = n_ep * CAP
    vmem = pl.BlockSpec(memory_space=pltpu.VMEM)
    hbm = pl.BlockSpec(memory_space=pl.ANY)
    dma = lambda *s: pltpu.SemaphoreType.DMA(s)
    buf = lambda *s: pltpu.VMEM(s, BF16)
    return pl.pallas_call(
        functools.partial(moe_kernel, n_ep),
        out_shape=jax.ShapeDtypeStruct((seqs, width), BF16),
        in_specs=[vmem] * 5 + [hbm] * 3,
        out_specs=vmem,
        scratch_shapes=[
            buf(*gate.shape), buf(*up.shape), buf(*down.shape),
            buf(seqs, width), buf(seqs, width), buf(seqs, width),
            buf(EXPERTS, block, quarter),
            buf(n_ep, 2, block, quarter),
            buf(count, width), buf(count, ff),
            buf(n_ep // GROUP, GROUP * block, quarter),
            buf(n_ep, block, quarter), buf(n_ep, block, quarter),
            buf(n_ep, block, quarter), buf(n_ep, block, quarter),
            buf(max(1, pieces - 1), EXPERTS, block, quarter),
            buf(EXPERTS, block, quarter), buf(EXPERTS, block, quarter),
            dma(3), dma(2), dma(EXPERTS), dma(max(1, EXPERTS * (pieces - 1))), dma(n_ep),
            dma(n_ep, 2), dma(pieces), dma(pieces),
            dma(max(1, pieces - 1), EXPERTS), dma(max(1, pieces - 1), EXPERTS),
            dma(EXPERTS), dma(EXPERTS), dma(2),
        ],
        compiler_params=pltpu.CompilerParams(
            collective_id=0, has_side_effects=True, vmem_limit_bytes=60 * 1024 * 1024
        ),
        name="experts",
    )(partial, tokens, expert_gain.reshape(1, width), routes, route_weights, gate, up, down)


def on_device(
    n_ep, tokens, lengths, key_cache, value_cache, gate_cache, mix_gain, query_weight, key_weight,
    value_weight, forget_weight, out_weight, expert_gain, routes, route_weights, expert_gate,
    expert_up, expert_down,
):
    partial = attention(
        tokens, lengths, key_cache, value_cache, gate_cache, mix_gain, query_weight, key_weight,
        value_weight, forget_weight, out_weight,
    )
    return moe(n_ep, partial, tokens, expert_gain, routes, route_weights,
               expert_gate, expert_up, expert_down)


def solution(mesh):
    return jax.shard_map(
        functools.partial(on_device, mesh.shape["ep"]),
        mesh=mesh,
        in_specs=(
            P("ep", None),
            P("ep"),
            P("ep", None, "tp"),
            P("ep", None, "tp"),
            P("ep", "tp", None),
            P(),
            P(None, "tp"),
            P(None, "tp"),
            P(None, "tp"),
            P(None, "tp"),
            P("tp", None),
            P(),
            P("ep", None),
            P("ep", None),
            P(None, ("ep", "tp")),
            P(None, ("ep", "tp")),
            P(("ep", "tp"), None),
        ),
        out_specs=P("ep", None),
        check_vma=False,
    )
```

time: 169 us -> 68.7 us (0.41)
  Pallas kernels: 0 us -> 56.4 us
  waiting for transfers between devices: 40.8 us -> 0 us
  matrix products: 34.1 us -> 0 us
  blocking collectives: 26.7 us -> 0 us
  local copies, waits for them, and re-layouts: 33.9 us -> 11.8 us
  between operations: 13.7 us -> 0.05 us
  other arithmetic: 11.7 us -> 0 us
  starting transfers between devices: 6.82 us -> 0 us
    pallas_call x0 -> x2, Pallas kernels: none -> 56.4 us  [the longest x1 39.3 us: moe(): pl.pallas_call(functools.partial(moe_kernel, n_ep), out_shape=jax.ShapeDt...]
    dot_general x11 -> x0, matrix products: 34.1 us -> none  [the longest x1 10.9 us: expert_work(): jnp.dot(hidden, expert_down, preferred_element_type=jnp.float32)]
    all_to_all x1 -> x0, blocking collectives: 22.1 us -> none  [on_device(): lax.all_to_all(outgoing_half, 'ep', split_axis=0, concat_axis=0, tiled=True)]
    psum x1 -> x0, waiting for transfers between devices: 20.2 us -> none  [on_device(): lax.psum(partial_out, 'tp').astype(jnp.float32)]
    all_to_all x1 -> x0, waiting for transfers between devices: 13.8 us -> none  [on_device(): lax.all_to_all(share, 'ep', split_axis=0, concat_axis=0, tiled=True)]
    unnamed x23 -> x24, local copies, waits for them, and re-layouts: 25.3 us -> 11.8 us
    all_to_all x1 -> x0, starting transfers between devices: 6.78 us -> none  [on_device(): lax.all_to_all(share, 'ep', split_axis=0, concat_axis=0, tiled=True)]
    reduce_scatter x1 -> x0, waiting for transfers between devices: 6.77 us -> none  [on_device(): lax.psum_scatter(partial_rows, 'tp', scatter_dimension=2, tiled=True)]
  transfers between devices with their start and end apart: 3 -> 0, of which waited for: 3 -> 0; matrix products, arithmetic and copies ran while one was open for 1% -> 0% of each run, Pallas kernels for 0% -> 0%
where the time goes in v1:
time: 68.7 us; the launch traced here: 68.2 us
  Pallas kernels  56.4 us (82%)
  local copies, waits for them, and re-layouts  11.8 us (17%)
    pallas_call x1, Pallas kernels, moe(): pl.pallas_call(functools.partial(moe_kernel, n_ep), out_shape=jax.ShapeDt...  39.3 us
    pallas_call x1, Pallas kernels, attention(): pl.pallas_call(attention_kernel, grid=(seqs // STEP_SEQS,), out_shape=jax...  17.1 us
    unnamed x24, local copies, waits for them, and re-layouts  11.8 us

profile of v1, /device:TPU:0, one launch (start us, length us, event | category | flops | bytes accessed | tf_op | source)
XLA Modules:
  0.0 68.2 jit_solution(10131396635935575066)
XLA Ops:
  0.0 1.0 %copy.18.wf_ref = bf16[2048,8]{1,0:T(8,128)(2,1)S(1)} copy(bf16[2048,8]{0,1:T(8,128)(2,1)} %param.26) | data formatting | bytes 65536 | tf_op args[9]
  1.0 0.0 copy-start
  1.0 1.6 %copy-done = bf16[2048,512]{1,0:T(8,128)(2,1)S(1)} copy-done((bf16[2048,512]{1,0:T(8,128)(2,1)S(1)}, bf16[2048,512]{1,0:T(8,128)(2,1)}, u32[]{:S(2)}) %copy-start) | copy-done | bytes 2097176
  2.6 1.2 %copy-done.1 = f32[32,8,1024]{2,1,0:T(8,128)S(1)} copy-done((f32[32,8,1024]{2,1,0:T(8,128)S(1)}, f32[32,8,1024]{2,1,0:T(8,128)}, u32[]{:S(2)}) %copy-start.1) | copy-done | bytes 1048600
  3.9 0.0 copy-start.2
  3.9 0.9 %copy-done.2 = bf16[32,2048]{1,0:T(8,128)(2,1)S(1)} copy-done((bf16[32,2048]{1,0:T(8,128)(2,1)S(1)}, bf16[32,2048]{1,0:T(8,128)(2,1)}, u32[]{:S(2)}) %copy-start.2) | copy-done | bytes 131096
  4.8 1.0 %copy-done.4 = bf16[2048,128]{1,0:T(8,128)(2,1)S(1)} copy-done((bf16[2048,128]{1,0:T(8,128)(2,1)S(1)}, bf16[2048,128]{1,0:T(8,128)(2,1)}, u32[]{:S(2)}) %copy-start.4) | copy-done | bytes 524312
  5.8 0.0 copy-start.5
  5.8 1.0 %copy-done.5 = bf16[2048,128]{1,0:T(8,128)(2,1)S(1)} copy-done((bf16[2048,128]{1,0:T(8,128)(2,1)S(1)}, bf16[2048,128]{1,0:T(8,128)(2,1)}, u32[]{:S(2)}) %copy-start.5) | copy-done | bytes 524312
  6.8 0.0 copy-start.6
  6.8 0.7 %copy-done.6 = f32[2048]{0:T(1024)S(1)} copy-done((f32[2048]{0:T(1024)S(1)}, f32[2048]{0:T(1024)}, u32[]{:S(2)}) %copy-start.6) | copy-done | bytes 8216
  7.5 0.0 copy-start.7
  7.5 0.7 copy-done.7
  8.2 0.0 copy-start.8
  8.2 0.0 copy-start.9
  8.2 17.1 %attention.1.part_ref = bf16[32,2048]{1,0:T(8,128)(2,1)S(1)} custom-call(s32[32]{0:T(128)S(1)} %copy-done.7, bf16[32,2048]{1,0:T(8,128)(2,1)S(1)} %copy-done.2, f32[1,2048]{1,0:T(1,128)S(1)} %bitcast.2, bf16[2048,512]{1,0:T(8,128)(2,1)S(1)} %copy-done, bf16[2048,128]{1,0:T(8,128)(2,1)S(1)} %copy-done.4, bf16[2048,128]{1,0:T(8,128)(2,1)S(1)} %copy-done.5, ...), custom_call_target="tpu_custom_call" | custom-call | tf_op jit(solution)/shard_map/attention/pallas_call | solution.py:106
  25.3 0.0 copy-start.3
  25.3 0.6 copy-done.3
  26.0 0.0 copy-done.8
  26.0 0.7 %copy.19.routes_ref = s32[32,2]{1,0:T(8,128)} copy(s32[32,2]{0,1:T(2,128)S(1)} %copy-done.8) | data formatting | bytes 512 | tf_op args[12]
  26.7 0.0 copy-done.9
  26.7 0.7 %copy.20.rw_ref = f32[32,2]{1,0:T(8,128)} copy(f32[32,2]{0,1:T(2,128)S(1)} %copy-done.9) | data formatting | bytes 512 | tf_op args[13]
  27.4 39.3 %experts.1 = bf16[32,2048]{1,0:T(8,128)(2,1)} custom-call(bf16[32,2048]{1,0:T(8,128)(2,1)} %copy-done.3, bf16[32,2048]{1,0:T(8,128)(2,1)} %tok_ref.3, f32[1,2048]{1,0:T(1,128)} %bitcast.3, s32[32,2]{1,0:T(8,128)} %copy.19.routes_ref, f32[32,2]{1,0:T(8,128)} %copy.20.rw_ref, bf16[2048,2048]{1,0:T(8,128)(2,1)} %wg_hbm.1, bf16[2048,2048]{1,0:T(8,128)(2,1)} %wu_hbm.1, ...), custom_call_target="tpu_custom_call" | custom-call | tf_op jit(solution)/shard_map/experts/pallas_call | solution.py:372
  66.7 1.6 %copy.22 = bf16[32,2048]{1,0:T(8,128)(2,1)} copy(bf16[32,2048]{1,0:T(8,128)(2,1)} %experts.1) | data formatting | bytes 262144
  (2 shorter events, 0.0 us)
Async XLA Ops:
  1.0 1.6 %copy-start = (bf16[2048,512]{1,0:T(8,128)(2,1)S(1)}, bf16[2048,512]{1,0:T(8,128)(2,1)}, u32[]{:S(2)}) copy-start(bf16[2048,512]{1,0:T(8,128)(2,1)} %wq_ref.1) | copy-start | bytes 6291460
  2.6 1.2 %copy-start.1 = (f32[32,8,1024]{2,1,0:T(8,128)S(1)}, f32[32,8,1024]{2,1,0:T(8,128)}, u32[]{:S(2)}) copy-start(f32[32,8,1024]{2,1,0:T(8,128)} %g_ref.1) | copy-start | bytes 3145732
  3.9 0.9 %copy-start.2 = (bf16[32,2048]{1,0:T(8,128)(2,1)S(1)}, bf16[32,2048]{1,0:T(8,128)(2,1)}, u32[]{:S(2)}) copy-start(bf16[32,2048]{1,0:T(8,128)(2,1)} %tok_ref.3) | copy-start | bytes 393220
  4.8 1.0 %copy-start.4 = (bf16[2048,128]{1,0:T(8,128)(2,1)S(1)}, bf16[2048,128]{1,0:T(8,128)(2,1)}, u32[]{:S(2)}) copy-start(bf16[2048,128]{1,0:T(8,128)(2,1)} %wk_ref.1) | copy-start | bytes 1572868
  5.8 1.0 %copy-start.5 = (bf16[2048,128]{1,0:T(8,128)(2,1)S(1)}, bf16[2048,128]{1,0:T(8,128)(2,1)}, u32[]{:S(2)}) copy-start(bf16[2048,128]{1,0:T(8,128)(2,1)} %wv_ref.1) | copy-start | bytes 1572868
  6.8 0.7 %copy-start.6 = (f32[2048]{0:T(1024)S(1)}, f32[2048]{0:T(1024)}, u32[]{:S(2)}) copy-start(f32[2048]{0:T(1024)} %param.22) | copy-start | bytes 24580
  7.5 0.7 copy-start.7
  8.2 17.8 %copy-start.8 = (s32[32,2]{0,1:T(2,128)S(1)}, s32[32,2]{0,1:T(2,128)}, u32[]{:S(2)}) copy-start(s32[32,2]{0,1:T(2,128)} %param.29) | copy-start | bytes 772
  8.2 18.5 %copy-start.9 = (f32[32,2]{0,1:T(2,128)S(1)}, f32[32,2]{0,1:T(2,128)}, u32[]{:S(2)}) copy-start(f32[32,2]{0,1:T(2,128)} %param.30) | copy-start | bytes 772
  25.3 0.7 copy-start.3

commit v2 on v1

--- a/solution.py
+++ b/solution.py
@@ -12,7 +12,7 @@
 CAP = 12
 QUARTERS = 4
 GROUP = 4
-STEP_SEQS = 4
+STEP_SEQS = 8
 MESH = pl.DeviceIdType.MESH
 F32 = jnp.float32
 BF16 = jnp.bfloat16
@@ -25,115 +25,93 @@
     return floats * lax.rsqrt(jnp.mean(floats * floats, axis=-1, keepdims=True) + eps) * gain
 
 
-def attention_kernel(
-    len_ref, tok_ref, gain_ref, wq_ref, wk_ref, wv_ref, wf_ref, wo_ref, k_ref, v_ref, g_ref,
-    out_ref, q_sc, lg_sc, kn_sc, vn_sc, mix_sc,
-):
-    step = pl.program_id(0)
+def project(tok_ref, gain_ref, wq_ref, wk_ref, wv_ref, wf_ref, q_sc, lg_sc, kn_sc, vn_sc, heads):
     seqs = tok_ref.shape[0]
-    heads = g_ref.shape[1]
-    lanes = k_ref.shape[2]
-    positions = k_ref.shape[1]
+    lanes = wk_ref.shape[1]
     group = heads // (lanes // HD)
     per_slice = lanes // HD
     lane = lax.broadcasted_iota(jnp.int32, (seqs, lanes), 1)
-
-    @pl.when(step == 0)
-    def _():
-        x = normed(tok_ref[...], gain_ref[...]).astype(BF16)
-        q = jnp.dot(x, wq_ref[...], preferred_element_type=F32).astype(BF16).astype(F32)
-        kn_sc[...] = jnp.dot(x, wk_ref[...], preferred_element_type=F32).astype(BF16).astype(F32)
-        vn_sc[...] = jnp.dot(x, wv_ref[...], preferred_element_type=F32).astype(BF16).astype(F32)
-        gates = jnp.dot(x, wf_ref[...], preferred_element_type=F32)
-        gates = jnp.minimum(gates, 0.0) - jnp.log1p(jnp.exp(-jnp.abs(gates)))
-        for h in range(heads):
-            base = (h // per_slice) * lanes
-            part = q[:, base:base + lanes]
-            at, want = h % per_slice, h // group
+    x = normed(tok_ref[...], gain_ref[...]).astype(BF16)
+    gates = lax.dot_general(x, wf_ref[...], (((1,), (1,)), ((), ())), preferred_element_type=F32)
+    gates = jnp.minimum(gates, 0.0) - jnp.log1p(jnp.exp(-jnp.abs(gates)))
+    q = jnp.dot(x, wq_ref[...], preferred_element_type=F32).astype(BF16).astype(F32)
+    kn_sc[...] = jnp.dot(x, wk_ref[...], preferred_element_type=F32).astype(BF16).astype(F32)
+    vn_sc[...] = jnp.dot(x, wv_ref[...], preferred_element_type=F32).astype(BF16).astype(F32)
+    for h in range(heads):
+        base = (h // per_slice) * lanes
+        part = q[:, base:base + lanes]
+        at, want = h % per_slice, h // group
+        if at != want:
+            part = pltpu.roll(part, (want - at) * HD % lanes, 1)
+        part = jnp.where(lane // HD == want, part, 0.0)
+        q_sc[:, h, :] = part
+        lg_sc[:, h, :] = jnp.broadcast_to(gates[:, h:h + 1], (seqs, lanes))
+
+
+def attend(base, len_ref, k_ref, v_ref, g_ref, q_sc, lg_sc, kn_sc, vn_sc, mix_sc):
+    heads, positions = g_ref.shape[1:]
+    pos = lax.broadcasted_iota(jnp.int32, (heads, positions), 1)
+    factor = HD ** (-0.5)
+    group = [base + j for j in range(STEP_SEQS)]
+    lengths = [len_ref[s] for s in group]
+    queries = [q_sc[s] for s in group]
+    scores = [
+        lax.dot_general(
+            q.astype(BF16), k_ref[s], (((1,), (1,)), ((), ())), preferred_element_type=F32
+        )
+        for s, q in zip(group, queries)
+    ]
+    latest = [
+        jnp.sum(jnp.where(pos == n - 1, g_ref[s], 0.0), axis=-1, keepdims=True)
+        for s, n in zip(group, lengths)
+    ]
+    own = [
+        jnp.sum(q * kn_sc[pl.ds(s, 1), :], axis=-1, keepdims=True) * factor
+        for s, q in zip(group, queries)
+    ]
+    scores = [
+        jnp.where(pos < n, c * factor + (l + lg_sc[s][:, 0:1]) - g_ref[s], -jnp.inf)
+        for s, n, c, l in zip(group, lengths, scores, latest)
+    ]
+    top = [jnp.maximum(jnp.max(c, axis=-1, keepdims=True), o) for c, o in zip(scores, own)]
+    raised = [jnp.exp(c - m) for c, m in zip(scores, top)]
+    own_raised = [jnp.exp(o - m) for o, m in zip(own, top)]
+    inverse = [
+        1.0 / (jnp.sum(r, axis=-1, keepdims=True) + o) for r, o in zip(raised, own_raised)
+    ]
+    weights = [(r * i).astype(BF16) for r, i in zip(raised, inverse)]
+    mixed = [
+        jnp.dot(w, v_ref[s], preferred_element_type=F32) for s, w in zip(group, weights)
+    ]
+    for s, m, o, i in zip(group, mixed, own_raised, inverse):
+        mix_sc[s] = m + (o * i).astype(BF16).astype(F32) * vn_sc[pl.ds(s, 1), :]
+
+
+def joined_heads(mix_sc):
+    seqs, heads, lanes = mix_sc.shape
+    per_slice = lanes // HD
+    group = heads // per_slice
+    lane = lax.broadcasted_iota(jnp.int32, (seqs, lanes), 1)
+    pieces = []
+    for base in range(0, heads, per_slice):
+        joined = None
+        for h in range(base, base + per_slice):
+            part = mix_sc[:, h, :]
+            at, want = h // group, h % per_slice
             if at != want:
                 part = pltpu.roll(part, (want - at) * HD % lanes, 1)
-            part = jnp.where(lane // HD == want, part, 0.0)
-            q_sc[:, h, :] = part
-            lg_sc[:, h, :] = jnp.broadcast_to(gates[:, h:h + 1], (seqs, lanes))
-
-    pos = lax.broadcasted_iota(jnp.int32, (heads, positions), 1)
-    factor = HD ** (-0.5)
-    for j in range(k_ref.shape[0]):
-        s = step * k_ref.shape[0] + j
-        length = len_ref[s]
-        q = q_sc[s]
-        g = g_ref[j]
-        scores = lax.dot_general(
-            q.astype(BF16), k_ref[j], (((1,), (1,)), ((), ())), preferred_element_type=F32
-        ) * factor
-        latest = jnp.sum(jnp.where(pos == length - 1, g, 0.0), axis=-1, keepdims=True)
-        scores = scores + (latest + lg_sc[s][:, 0:1]) - g
-        scores = jnp.where(pos < length, scores, -jnp.inf)
-        own = jnp.sum(q * kn_sc[pl.ds(s, 1), :], axis=-1, keepdims=True) * factor
-        top = jnp.maximum(jnp.max(scores, axis=-1, keepdims=True), own)
-        raised = jnp.exp(scores - top)
-        own_raised = jnp.exp(own - top)
-        inverse = 1.0 / (jnp.sum(raised, axis=-1, keepdims=True) + own_raised)
-        weights = (raised * inverse).astype(BF16)
-        own_weight = (own_raised * inverse).astype(BF16).astype(F32)
-        mix_sc[s] = (
-            jnp.dot(weights, v_ref[j], preferred_element_type=F32)
-            + own_weight * vn_sc[pl.ds(s, 1), :]
-        )
-
-    @pl.when(step == pl.num_programs(0) - 1)
-    def _():
-        pieces = []
-        for base in range(0, heads, per_slice):
-            joined = None
-            for h in range(base, base + per_slice):
-                part = mix_sc[:, h, :]
-                at, want = h // group, h % per_slice
-                if at != want:
-                    part = pltpu.roll(part, (want - at) * HD % lanes, 1)
-                joined = part if joined is None else jnp.where(lane // HD == want, part, joined)
-            pieces.append(joined.astype(BF16))
-        mixed = jnp.concatenate(pieces, axis=1)
-        out_ref[...] = jnp.dot(mixed, wo_ref[...], preferred_element_type=F32).astype(BF16)
-
-
-def attention(tokens, lengths, key_cache, value_cache, gate_cache, mix_gain, wq, wk, wv, wf, wo):
-    seqs, width = tokens.shape
-    _, positions, lanes = key_cache.shape
-    heads = gate_cache.shape[1]
-    whole = lambda a: pl.BlockSpec(a.shape, lambda i: (0,) * a.ndim)
-    gain = mix_gain.reshape(1, width)
-    return pl.pallas_call(
-        attention_kernel,
-        grid=(seqs // STEP_SEQS,),
-        out_shape=jax.ShapeDtypeStruct((seqs, width), BF16),
-        in_specs=[pl.BlockSpec(memory_space=pltpu.SMEM)]
-        + [whole(a) for a in (tokens, gain, wq, wk, wv, wf, wo)]
-        + [
-            pl.BlockSpec((STEP_SEQS, positions, lanes), lambda i: (i, 0, 0)),
-            pl.BlockSpec((STEP_SEQS, positions, lanes), lambda i: (i, 0, 0)),
-            pl.BlockSpec((STEP_SEQS, heads, positions), lambda i: (i, 0, 0)),
-        ],
-        out_specs=pl.BlockSpec((seqs, width), lambda i: (0, 0)),
-        scratch_shapes=[
-            pltpu.VMEM((seqs, heads, lanes), F32),
-            pltpu.VMEM((seqs, heads, lanes), F32),
-            pltpu.VMEM((seqs, lanes), F32),
-            pltpu.VMEM((seqs, lanes), F32),
-            pltpu.VMEM((seqs, heads, lanes), F32),
-        ],
-        compiler_params=pltpu.CompilerParams(
-            dimension_semantics=("arbitrary",), vmem_limit_bytes=48 * 1024 * 1024
-        ),
-        name="attention",
-    )(lengths, tokens, gain, wq, wk, wv, wf, wo, key_cache, value_cache, gate_cache)
+            joined = part if joined is None else jnp.where(lane // HD == want, part, joined)
+        pieces.append(joined.astype(BF16))
+    return jnp.concatenate(pieces, axis=1)
 
 
 def moe_kernel(
-    n_ep, part_ref, tok_ref, gain_ref, routes_ref, rw_ref, wg_hbm, wu_hbm, wd_hbm, out_ref,
-    wg, wu, wd, peer_part, residual, normal, outgoing, rows, x_sc, h_sc, stage, s_other, s_own,
+    n_ep, len_ref, mix_gain_ref, gain_ref, routes_ref, rw_ref, tok_hbm, wq_hbm, wk_hbm, wv_hbm,
+    wf_hbm, k_hbm, v_hbm, g_hbm, wo_hbm, wg_hbm, wu_hbm, wd_hbm, out_ref,
+    tok_ref, wq, wk, wv, wf, keys, values, gates, wo, wg, wu, wd,
+    q_sc, lg_sc, kn_sc, vn_sc, mix_sc, part_ref, peer_part, residual, normal, outgoing, rows, x_sc, h_sc, stage, s_other, s_own,
     t_in, blocks, u_in, finals, returned,
-    w_sem, part_sem, col_send, fan_send, mate_send, row_recv, t_send, t_recv, u_send, u_recv,
+    in_sem, kv_sem, w_sem, part_sem, col_send, fan_send, mate_send, row_recv, t_send, t_recv, u_send, u_recv,
     ret_send, ret_recv, out_sem,
 ):
     me = lax.axis_index("ep")
@@ -153,6 +131,28 @@
     def peer(i):
         return lax.rem(p + i, pieces)
 
+    head_copies = [
+        pltpu.make_async_copy(src, dst, in_sem.at[i])
+        for i, (src, dst) in enumerate((
+            (tok_hbm, tok_ref), (wf_hbm, wf), (wq_hbm, wq), (wk_hbm, wk), (wv_hbm, wv),
+            (wo_hbm, wo),
+        ))
+    ]
+    for copy in head_copies[:-1]:
+        copy.start()
+    steps = seqs // STEP_SEQS
+
+    def cache_copies(i):
+        at = pl.ds(pl.multiple_of(i * STEP_SEQS, STEP_SEQS), STEP_SEQS)
+        return [
+            pltpu.make_async_copy(src.at[at], dst.at[at], kv_sem.at[n, i])
+            for n, (src, dst) in enumerate(((k_hbm, keys), (g_hbm, gates), (v_hbm, values)))
+        ]
+
+    for i in range(steps):
+        for copy in cache_copies(i):
+            copy.start()
+    head_copies[-1].start()
     weight_copies = [
         pltpu.make_async_copy(src, dst, w_sem.at[i])
         for i, (src, dst) in enumerate(((wg_hbm, wg), (wu_hbm, wu), (wd_hbm, wd)))
@@ -166,6 +166,22 @@
         pl.semaphore_signal(barrier, inc=1, device_id=(e * pieces + peer(i), t), device_id_type=MESH)
     for k in range(1, EXPERTS):
         pl.semaphore_signal(barrier, inc=1, device_id=(column(k) * pieces + p, t), device_id_type=MESH)
+
+    for copy in head_copies[:-1]:
+        copy.wait()
+    project(tok_ref, mix_gain_ref, wq, wk, wv, wf, q_sc, lg_sc, kn_sc, vn_sc, gates.shape[1])
+
+    @pl.loop(0, steps)
+    def _(i):
+        for copy in cache_copies(i):
+            copy.wait()
+        attend(i * STEP_SEQS, len_ref, keys, values, gates, q_sc, lg_sc, kn_sc, vn_sc, mix_sc)
+
+    head_copies[-1].wait()
+    part_ref[...] = jnp.dot(
+        joined_heads(mix_sc), wo[...], preferred_element_type=F32
+    ).astype(BF16)
+
     pl.semaphore_wait(barrier, 1 + (pieces - 1) + (EXPERTS - 1))
 
     def send(src, dst, send_sem, recv_sem, device):
@@ -186,25 +202,25 @@
 
     block = QUARTERS * CAP
     columns = EXPERTS * block
-    col = lax.broadcasted_iota(jnp.int32, (seqs, columns), 1)
-    col_expert = col // block
-    col_slot = lax.rem(col, CAP)
-    r0, r1 = routes_ref[:, 0:1], routes_ref[:, 1:2]
-    first, second = r0 == col_expert, r1 == col_expert
+    spread = (columns, QUARTERS * seqs)
+    row = lax.broadcasted_iota(jnp.int32, spread, 0)
+    row_expert = row // block
+    row_slot = lax.rem(row, CAP)
+    same_quarter = lax.rem(row, block) // CAP == lax.broadcasted_iota(jnp.int32, spread, 1) // seqs
+    tiled = lambda a: jnp.concatenate([a] * QUARTERS, axis=1)
+    routes = tiled(routes_ref[...])
+    shares = tiled(rw_ref[...])
+    first, second = routes[0:1] == row_expert, routes[1:2] == row_expert
     named = jnp.where(first | second, 1.0, 0.0)
+    square = (QUARTERS * seqs, QUARTERS * seqs)
+    earlier = lax.broadcasted_iota(jnp.int32, square, 0)
     before = jnp.where(
-        lax.broadcasted_iota(jnp.int32, (seqs, seqs), 1)
-        < lax.broadcasted_iota(jnp.int32, (seqs, seqs), 0), 1.0, 0.0,
+        earlier < lax.rem(lax.broadcasted_iota(jnp.int32, square, 1), seqs), 1.0, 0.0
     )
-    slot = jnp.dot(before.astype(BF16), named.astype(BF16), preferred_element_type=F32)
-    chosen = jnp.where(slot == col_slot.astype(F32), named, 0.0)
-    weight = jnp.where(first, rw_ref[:, 0:1], jnp.where(second, rw_ref[:, 1:2], 0.0)) * chosen
-    col_quarter = lax.rem(col, block) // CAP
-    spread = lambda a: jnp.concatenate(
-        [jnp.where(col_quarter == q, a, 0.0) for q in range(QUARTERS)], axis=0
-    )
-    dispatch = spread(chosen).astype(BF16)
-    weight = spread(weight)
+    slot = jnp.dot(named.astype(BF16), before.astype(BF16), preferred_element_type=F32)
+    chosen = jnp.where(same_quarter & (slot == row_slot.astype(F32)), named, 0.0)
+    weight = jnp.where(first, shares[0:1], jnp.where(second, shares[1:2], 0.0)) * chosen
+    dispatch = chosen.astype(BF16)
     weight_high = weight.astype(BF16)
     weight_low = (weight - weight_high.astype(F32)).astype(BF16)
 
@@ -232,7 +248,7 @@
         [mine[:, q * quarter:(q + 1) * quarter] for q in range(QUARTERS)], axis=0
     )
     outgoing[...] = lax.dot_general(
-        dispatch, stacked, (((0,), (0,)), ((), ())), preferred_element_type=F32
+        dispatch, stacked, (((1,), (0,)), ((), ())), preferred_element_type=F32
     ).astype(BF16).reshape(EXPERTS, block, quarter)
 
     own_row = p * EXPERTS + e
@@ -340,9 +356,10 @@
     for a in inbound:
         arrived(returned.at[a], ret_send.at[0], ret_recv.at[a])
     back = returned[...].reshape(columns, quarter)
+    over_rows = (((0,), (0,)), ((), ()))
     mixture = (
-        jnp.dot(weight_high, back, preferred_element_type=F32)
-        + jnp.dot(weight_low, back, preferred_element_type=F32)
+        lax.dot_general(weight_high, back, over_rows, preferred_element_type=F32)
+        + lax.dot_general(weight_low, back, over_rows, preferred_element_type=F32)
     )
     for q in range(QUARTERS):
         at = pl.ds(pl.multiple_of(start + q * quarter, quarter), quarter)
@@ -357,26 +374,41 @@
         copy.wait_send()
 
 
-def moe(n_ep, partial, tokens, expert_gain, routes, route_weights, gate, up, down):
+def on_device(
+    n_ep, tokens, lengths, key_cache, value_cache, gate_cache, mix_gain, query_weight, key_weight,
+    value_weight, forget_weight, out_weight, expert_gain, routes, route_weights, expert_gate,
+    expert_up, expert_down,
+):
     seqs, width = tokens.shape
+    heads = gate_cache.shape[1]
+    lanes = key_cache.shape[2]
     pieces = n_ep // EXPERTS
     half = width // 2
     quarter = half // QUARTERS
     block = QUARTERS * CAP
-    ff = gate.shape[1]
+    ff = expert_gate.shape[1]
     count = n_ep * CAP
     vmem = pl.BlockSpec(memory_space=pltpu.VMEM)
+    smem = pl.BlockSpec(memory_space=pltpu.SMEM)
     hbm = pl.BlockSpec(memory_space=pl.ANY)
     dma = lambda *s: pltpu.SemaphoreType.DMA(s)
     buf = lambda *s: pltpu.VMEM(s, BF16)
+    copied = (
+        tokens, query_weight, key_weight, value_weight, forget_weight.T, key_cache, value_cache,
+        gate_cache, out_weight, expert_gate, expert_up, expert_down,
+    )
     return pl.pallas_call(
         functools.partial(moe_kernel, n_ep),
         out_shape=jax.ShapeDtypeStruct((seqs, width), BF16),
-        in_specs=[vmem] * 5 + [hbm] * 3,
+        in_specs=[smem] + [vmem] * 4 + [hbm] * len(copied),
         out_specs=vmem,
-        scratch_shapes=[
-            buf(*gate.shape), buf(*up.shape), buf(*down.shape),
-            buf(seqs, width), buf(seqs, width), buf(seqs, width),
+        scratch_shapes=[pltpu.VMEM(a.shape, a.dtype) for a in copied] + [
+            pltpu.VMEM((seqs, heads, lanes), F32),
+            pltpu.VMEM((seqs, heads, lanes), F32),
+            pltpu.VMEM((seqs, lanes), F32),
+            pltpu.VMEM((seqs, lanes), F32),
+            pltpu.VMEM((seqs, heads, lanes), F32),
+            buf(seqs, width), buf(seqs, width), buf(seqs, width), buf(seqs, width),
             buf(EXPERTS, block, quarter),
             buf(n_ep, 2, block, quarter),
             buf(count, width), buf(count, ff),
@@ -385,29 +417,18 @@
             buf(n_ep, block, quarter), buf(n_ep, block, quarter),
             buf(max(1, pieces - 1), EXPERTS, block, quarter),
             buf(EXPERTS, block, quarter), buf(EXPERTS, block, quarter),
+            dma(6), dma(3, seqs // STEP_SEQS),
             dma(3), dma(2), dma(EXPERTS), dma(max(1, EXPERTS * (pieces - 1))), dma(n_ep),
             dma(n_ep, 2), dma(pieces), dma(pieces),
             dma(max(1, pieces - 1), EXPERTS), dma(max(1, pieces - 1), EXPERTS),
             dma(EXPERTS), dma(EXPERTS), dma(2),
         ],
         compiler_params=pltpu.CompilerParams(
-            collective_id=0, has_side_effects=True, vmem_limit_bytes=60 * 1024 * 1024
+            collective_id=0, has_side_effects=True, vmem_limit_bytes=67043328
         ),
-        name="experts",
-    )(partial, tokens, expert_gain.reshape(1, width), routes, route_weights, gate, up, down)
-
-
-def on_device(
-    n_ep, tokens, lengths, key_cache, value_cache, gate_cache, mix_gain, query_weight, key_weight,
-    value_weight, forget_weight, out_weight, expert_gain, routes, route_weights, expert_gate,
-    expert_up, expert_down,
-):
-    partial = attention(
-        tokens, lengths, key_cache, value_cache, gate_cache, mix_gain, query_weight, key_weight,
-        value_weight, forget_weight, out_weight,
-    )
-    return moe(n_ep, partial, tokens, expert_gain, routes, route_weights,
-               expert_gate, expert_up, expert_down)
+        name="layer",
+    )(lengths, mix_gain.reshape(1, width), expert_gain.reshape(1, width), routes.T,
+      route_weights.T, *copied)
 
 
 def solution(mesh):

time: 68.7 us -> 52.6 us (0.77)
  local copies, waits for them, and re-layouts: 11.8 us -> 1.57 us
  Pallas kernels: 56.4 us -> 50.8 us
    unnamed x24 -> x1, local copies, waits for them, and re-layouts: 11.8 us -> 1.57 us
    pallas_call x2 -> x1, Pallas kernels: 56.4 us -> 50.8 us  [on_device(): pl.pallas_call(functools.partial(moe_kernel, n_ep), out_shape=jax.ShapeDt...]
where the time goes in v2:
time: 52.6 us; the launch traced here: 52.4 us
  Pallas kernels  50.8 us (97%)
  local copies, waits for them, and re-layouts  1.57 us (3%)
    pallas_call x1, Pallas kernels, on_device(): pl.pallas_call(functools.partial(moe_kernel, n_ep), out_shape=jax.ShapeDt...  50.8 us
    unnamed x1, local copies, waits for them, and re-layouts  1.57 us

profile of v2, /device:TPU:0, one launch (start us, length us, event | category | flops | bytes accessed | tf_op | source)
XLA Modules:
  0.0 52.4 jit_solution(17876642781837061167)
XLA Ops:
  0.0 50.8 %layer.1 = bf16[32,2048]{1,0:T(8,128)(2,1)} custom-call(s32[32]{0:T(128)} %len_ref.1, f32[1,2048]{1,0:T(1,128)} %bitcast.6, f32[1,2048]{1,0:T(1,128)} %bitcast.7, s32[2,32]{1,0:T(2,128)} %bitcast.8, f32[2,32]{1,0:T(2,128)} %bitcast.9, bf16[32,2048]{1,0:T(8,128)(2,1)} %tok_hbm.1, bf16[2048,512]{1,0:T(8,128)(2,1)} %wq_hbm.1, bf16[2048,128]{1,0:T(8,128)(2,1)} %wk_hbm.1, ...), custom_call_target="tpu_custom_call" | custom-call | tf_op jit(solution)/shard_map/layer/pallas_call | solution.py:400
  50.8 1.6 %copy.19 = bf16[32,2048]{1,0:T(8,128)(2,1)} copy(bf16[32,2048]{1,0:T(8,128)(2,1)} %layer.1) | data formatting | bytes 262144

commit v3 on v2

--- a/solution.py
+++ b/solution.py
@@ -12,7 +12,7 @@
 CAP = 12
 QUARTERS = 4
 GROUP = 4
-STEP_SEQS = 8
+STEP_SEQS = 16
 MESH = pl.DeviceIdType.MESH
 F32 = jnp.float32
 BF16 = jnp.bfloat16
@@ -157,8 +157,6 @@
         pltpu.make_async_copy(src, dst, w_sem.at[i])
         for i, (src, dst) in enumerate(((wg_hbm, wg), (wu_hbm, wu), (wd_hbm, wd)))
     ]
-    for copy in weight_copies:
-        copy.start()
 
     barrier = pltpu.get_barrier_semaphore()
     pl.semaphore_signal(barrier, inc=1, device_id=mate, device_id_type=MESH)
@@ -177,6 +175,8 @@
             copy.wait()
         attend(i * STEP_SEQS, len_ref, keys, values, gates, q_sc, lg_sc, kn_sc, vn_sc, mix_sc)
 
+    for copy in weight_copies:
+        copy.start()
     head_copies[-1].wait()
     part_ref[...] = jnp.dot(
         joined_heads(mix_sc), wo[...], preferred_element_type=F32

time: 52.6 us -> 49.1 us (0.933)
  Pallas kernels: 50.8 us -> 47.3 us
    pallas_call x1, Pallas kernels: 50.8 us -> 47.3 us  [on_device(): pl.pallas_call(functools.partial(moe_kernel, n_ep), out_shape=jax.ShapeDt...]
where the time goes in v3:
time: 49.1 us; the launch traced here: 48.9 us
  Pallas kernels  47.3 us (96%)
  local copies, waits for them, and re-layouts  1.57 us (3%)
    pallas_call x1, Pallas kernels, on_device(): pl.pallas_call(functools.partial(moe_kernel, n_ep), out_shape=jax.ShapeDt...  47.3 us
    unnamed x1, local copies, waits for them, and re-layouts  1.57 us

profile of v3, /device:TPU:0, one launch (start us, length us, event | category | flops | bytes accessed | tf_op | source)
XLA Modules:
  0.0 48.9 jit_solution(3107311835106457585)
XLA Ops:
  0.0 47.3 %layer.1 = bf16[32,2048]{1,0:T(8,128)(2,1)} custom-call(s32[32]{0:T(128)} %len_ref.1, f32[1,2048]{1,0:T(1,128)} %bitcast.6, f32[1,2048]{1,0:T(1,128)} %bitcast.7, s32[2,32]{1,0:T(2,128)} %bitcast.8, f32[2,32]{1,0:T(2,128)} %bitcast.9, bf16[32,2048]{1,0:T(8,128)(2,1)} %tok_hbm.1, bf16[2048,512]{1,0:T(8,128)(2,1)} %wq_hbm.1, bf16[2048,128]{1,0:T(8,128)(2,1)} %wk_hbm.1, ...), custom_call_target="tpu_custom_call" | custom-call | tf_op jit(solution)/shard_map/layer/pallas_call | solution.py:400
  47.3 1.6 %copy.19 = bf16[32,2048]{1,0:T(8,128)(2,1)} copy(bf16[32,2048]{1,0:T(8,128)(2,1)} %layer.1) | data formatting | bytes 262144
